TPU v7x, 128 devices: a whole 4x4x4 slice. The times are simulated.
128 devices in a mesh: sp: 16 (over z, y), tp: 4 (over x), dp: 2 (over core).
Axes of the slice: x: 4, y: 4, z: 4, core: 2. Of those that a mesh axis runs over, the one named last changes fastest.
Arguments:
- latent: bfloat16 [2, 12288, 2048], P('dp', ('sp', 'tp')), may hold values from -3 to 3
- cond: bfloat16 [2, 2048], P('dp', 'sp'), may hold values from -6 to 6
- cond_ctx: bfloat16 [2048], P('sp'), may hold values from -6 to 6
- context: bfloat16 [2, 512, 2048], P('dp', 'sp'), may hold values from -6 to 6
- norm_gain: bfloat16 [2048], replicated, may hold values from 0.099609375 to 1.8984375
- mod_shift: bfloat16 [2048, 2048], P('sp', 'tp'), may hold values from -0.125 to 0.125
- mod_scale: bfloat16 [2048, 2048], P('sp', 'tp'), may hold values from -0.125 to 0.125
- mod_gate: bfloat16 [2048, 2048], P('sp', 'tp'), may hold values from -0.125 to 0.125
- w_query: bfloat16 [2048, 1024], P(None, 'tp'), may hold values from -0.125 to 0.125
- w_key: bfloat16 [2048, 256], P(None, 'tp'), may hold values from -0.125 to 0.125
- w_value: bfloat16 [2048, 256], P(None, 'tp'), may hold values from -0.125 to 0.125
- q_gain: bfloat16 [64], replicated, may hold values from 1 to 5.5
- k_gain: bfloat16 [64], replicated, may hold values from 1 to 5.5
- ctx_lift: float32 [16], P('tp'), may hold values from 1 to 3
- w_out: bfloat16 [1024, 2048], replicated, may hold values from -1.5 to 1.5
Outputs:
- mixed: bfloat16 [2, 12288, 2048], P('dp', ('sp', 'tp'))
All inputs are finite; a program needn't handle non-finite values.
Results may differ from a plain program's by a relative error of at most 0.009.
The roundings to bfloat16 on the way count: a program that leaves them out, or rounds other values in their place, can miss the bound.
Values may be sent and summed in bfloat16 or wider, within the bound.
A program may use at most 64 MiB of HBM per device.

v0:
```python
import jax
import jax.numpy as jnp
from jax import lax
from jax.sharding import Mesh
from jax.sharding import PartitionSpec as P

HD = 64
GRID_W = 128
SP_TP = ("sp_0", "sp_1", "tp")
SP = ("sp_0", "sp_1")
EPS = 1e-06
THETA = 10000.0


def by_axis(shard, axes):
    for axis in axes:
        shard = lax.psum(shard, axis)
    return shard


def laid_out(blocks, dim):
    blocks = jnp.moveaxis(blocks, 0, dim)
    lengths = blocks.shape
    return blocks.reshape(*lengths[:dim], lengths[dim] * lengths[dim + 1], *lengths[dim + 2 :])


def copy_for_each(shard, axis):
    copies = jnp.broadcast_to(shard, (lax.axis_size(axis), *shard.shape))
    return lax.all_to_all(copies, axis, split_axis=0, concat_axis=0, tiled=True)


def gather_directly(shard, axis, dim):
    return laid_out(copy_for_each(shard, axis), dim)


def side_by_side(arrays, axis, dim, along):
    ends, at = ([], 0)
    for a in arrays[:-1]:
        at += a.shape[along]
        ends.append(at)
    both = jnp.concatenate(arrays, axis=along)
    return tuple(jnp.split(lax.all_gather(both, axis, axis=dim, tiled=True), ends, axis=along))


def modulate(row_block, gain_vec, shift_rows, scale_rows):
    values = row_block.astype(jnp.float32)
    normed = (
        values
        * lax.rsqrt(jnp.mean(values * values, axis=-1, keepdims=True) + EPS)
        * gain_vec.astype(jnp.float32)
    )
    return (normed * (1.0 + scale_rows) + shift_rows).astype(jnp.bfloat16)


def head_norm(raw_proj, gain_vec):
    samples, tokens, width = raw_proj.shape
    pieces = raw_proj.reshape(samples, tokens, width // HD, HD)
    normed = (
        pieces
        * lax.rsqrt(jnp.mean(pieces * pieces, axis=-1, keepdims=True) + EPS)
        * gain_vec.astype(jnp.float32)
    )
    return normed.transpose(0, 2, 1, 3)


def rotate(vector, positions):
    pairs_count = vector.shape[-1] // 4
    grid_row = (positions // GRID_W).astype(jnp.float32)
    grid_col = (positions % GRID_W).astype(jnp.float32)
    inverse = THETA ** (-jnp.arange(pairs_count, dtype=jnp.float32) / pairs_count)
    angles = jnp.concatenate([grid_row[:, None] * inverse, grid_col[:, None] * inverse], axis=-1)
    cosine = jnp.cos(angles)
    sine_val = jnp.sin(angles)
    first_half = vector[..., 0::2]
    second_half = vector[..., 1::2]
    turned = jnp.stack(
        [
            first_half * cosine - second_half * sine_val,
            first_half * sine_val + second_half * cosine,
        ],
        axis=-1,
    )
    return turned.reshape(vector.shape)


def split_heads(rows):
    samples, tokens, width = rows.shape
    return rows.reshape(samples, tokens, width // HD, HD).transpose(0, 2, 1, 3)


def on_device(
    latent,
    cond,
    cond_ctx,
    context,
    norm_gain,
    mod_shift,
    mod_scale,
    mod_gate,
    w_query,
    w_key,
    w_value,
    q_gain,
    k_gain,
    ctx_lift,
    w_out,
):
    samples = latent.shape[0]
    active = jax.nn.silu(
        jnp.concatenate([cond, cond_ctx[None, :]], axis=0).astype(jnp.float32)
    ).astype(jnp.bfloat16)
    partial_mods = tuple(
        (
            jnp.dot(active, weight, preferred_element_type=jnp.float32)
            for weight in (mod_shift, mod_scale, mod_gate)
        )
    )
    col_width = mod_shift.shape[1]
    offset = lax.axis_index("tp") * col_width
    blank = jnp.zeros((active.shape[0], col_width * lax.axis_size("tp")), jnp.float32)
    placed = tuple(
        (lax.dynamic_update_slice(blank, term, (jnp.int32(0), offset)) for term in partial_mods)
    )
    shift_rows, scale_rows, gate_rows = jax.tree.map(lambda part: by_axis(part, SP_TP), placed)
    modulated = modulate(
        latent, norm_gain, shift_rows[:samples, None, :], scale_rows[:samples, None, :]
    )
    ctx_mod = modulate(context, norm_gain, shift_rows[samples], scale_rows[samples])
    q_width = w_query.shape[1]
    k_width = w_key.shape[1]
    w_joint = jnp.concatenate([w_query, w_key, w_value], axis=1)
    projected = jnp.einsum(
        "srd,dc->src",
        gather_directly(modulated, "tp", 1),
        w_joint,
        preferred_element_type=jnp.float32,
    )
    tokens = projected.shape[1]
    k_heads = k_width // HD
    group_size = q_width // k_width
    positions = lax.axis_index(SP) * tokens + jnp.arange(tokens, dtype=jnp.int32)
    queries = rotate(head_norm(projected[..., :q_width], q_gain), positions).astype(jnp.bfloat16)
    queries = queries.reshape(samples, k_heads, group_size, tokens, HD)
    key_rows = rotate(
        head_norm(projected[..., q_width : q_width + k_width], k_gain), positions
    ).astype(jnp.bfloat16)
    value_rows = split_heads(projected[..., q_width + k_width :].astype(jnp.bfloat16))
    ctx_proj = jnp.einsum(
        "srd,dc->src", ctx_mod, w_joint[:, q_width:], preferred_element_type=jnp.float32
    )
    ctx_keys = head_norm(ctx_proj[..., :k_width], k_gain).astype(jnp.bfloat16)
    ctx_values = split_heads(ctx_proj[..., k_width:].astype(jnp.bfloat16))
    lift_table = ctx_lift.reshape(1, k_heads, group_size, 1, 1)
    factor = HD ** (-0.5)

    def absorb(state_now, key_block, value_block, score_lift):
        best_old, weight_sum, accumulated = state_now
        scores = (
            jnp.einsum("skgtd,skrd->skgtr", queries, key_block, preferred_element_type=jnp.float32)
            * factor
            + score_lift
        )
        peak = jnp.maximum(best_old, jnp.max(scores, axis=-1))
        weights = jnp.exp(scores - peak[..., None])
        rescale = jnp.exp(best_old - peak)
        weight_sum = weight_sum * rescale + jnp.sum(weights, axis=-1)
        accumulated = accumulated * rescale[..., None] + jnp.einsum(
            "skgtr,skrd->skgtd",
            weights.astype(jnp.bfloat16),
            value_block,
            preferred_element_type=jnp.float32,
        )
        return (peak, weight_sum, accumulated)

    stat_shape = (samples, k_heads, group_size, tokens)
    state_now = (
        jnp.full(stat_shape, -1e30, jnp.float32),
        jnp.zeros(stat_shape, jnp.float32),
        jnp.zeros(stat_shape + (HD,), jnp.float32),
    )
    all_ctx_keys, all_ctx_values = side_by_side((ctx_keys, ctx_values), SP, 2, 0)
    state_now = absorb(state_now, all_ctx_keys, all_ctx_values, lift_table)
    key_piece, value_piece = side_by_side((key_rows, value_rows), SP, 2, 0)
    block_count = key_piece.shape[2] // tokens
    key_blocks = jnp.moveaxis(key_piece.reshape(samples, k_heads, block_count, tokens, HD), 2, 0)
    value_blocks = jnp.moveaxis(
        value_piece.reshape(samples, k_heads, block_count, tokens, HD), 2, 0
    )

    def step_block(carry, blocks):
        return (absorb(carry, blocks[0], blocks[1], 0.0), None)

    state_out, unused = lax.scan(step_block, state_now, (key_blocks, value_blocks))
    state_now = state_out
    best_old, weight_sum, accumulated = state_now
    attended = (accumulated / weight_sum[..., None]).astype(jnp.bfloat16)
    head_rows = attended.transpose(0, 3, 1, 2, 4).reshape(samples, tokens, q_width)
    projected_out = jnp.einsum(
        "srq,qd->srd",
        lax.all_to_all(head_rows, "tp", split_axis=1, concat_axis=2, tiled=True),
        w_out,
        preferred_element_type=jnp.float32,
    )
    return (latent.astype(jnp.float32) + gate_rows[:samples, None, :] * projected_out).astype(
        jnp.bfloat16
    )


def solution(mesh):
    torus = Mesh(
        mesh.devices.reshape(4, 4, mesh.shape["tp"], mesh.shape["dp"]), ("sp_0", "sp_1", "tp", "dp")
    )
    in_specs = (
        P("dp", SP_TP, None),
        P("dp", SP),
        P(SP),
        P("dp", SP, None),
        P(),
        P(SP, "tp"),
        P(SP, "tp"),
        P(SP, "tp"),
        P(None, "tp"),
        P(None, "tp"),
        P(None, "tp"),
        P(),
        P(),
        P("tp"),
        P(),
    )
    out_specs = P("dp", SP_TP, None)
    return jax.shard_map(
        on_device, mesh=torus, in_specs=in_specs, out_specs=out_specs, check_vma=False
    )
```

profile of v0, /device:TPU:0, one launch (start us, length us, event | category | flops | bytes accessed | tf_op | source)
XLA Modules:
  0.0 279.6 jit_solution(13613016184180509849)
XLA Ops:
  11.7 18.8 %all-reduce.2 = (f32[2,2048]{1,0:T(2,128)S(1)}, f32[2,2048]{1,0:T(2,128)S(1)}, f32[2,2048]{1,0:T(2,128)S(1)}) all-reduce(f32[2,2048]{1,0:T(2,128)S(1)} %convolution_dynamic-update-slice_fusion, f32[2,2048]{1,0:T(2,128)S(1)} %convolution_dynamic-update-slice_fusion.1, ...), channel_id=1, replica_groups=mesh['sp_0'=4,'sp_1'=4,'tp'=4,'dp'=2] {'sp_0'}, use_global_device_ids=true, to_apply=%region_7.8 | all-reduce | flops 12288 | bytes 98304 | tf_op jit(solution)/shard_map/psum | solution.py:17
  30.5 17.8 %all-reduce.1 = (f32[2,2048]{1,0:T(2,128)S(1)}, f32[2,2048]{1,0:T(2,128)S(1)}, f32[2,2048]{1,0:T(2,128)S(1)}) all-reduce(f32[2,2048]{1,0:T(2,128)S(1)} %get-tuple-element.93, f32[2,2048]{1,0:T(2,128)S(1)} %get-tuple-element.94, f32[2,2048]{1,0:T(2,128)S(1)} %get-tuple-element.95), channel_id=1, replica_groups=mesh['sp_0'=4,'sp_1'=4,'tp'=4,'dp'=2] {'sp_1'}, use_global_device_ids=true, to_apply=%region_8.9 | all-reduce | flops 12288 | bytes 98304 | tf_op jit(solution)/shard_map/psum | solution.py:17
  48.2 18.0 %all-reduce = (f32[2,2048]{1,0:T(2,128)S(1)}, f32[2,2048]{1,0:T(2,128)S(1)}, f32[2,2048]{1,0:T(2,128)}) all-reduce(f32[2,2048]{1,0:T(2,128)S(1)} %get-tuple-element.90, f32[2,2048]{1,0:T(2,128)S(1)} %get-tuple-element.91, f32[2,2048]{1,0:T(2,128)S(1)} %get-tuple-element.92), channel_id=1, replica_groups=mesh['sp_0'=4,'sp_1'=4,'tp'=4,'dp'=2] {'tp'}, use_global_device_ids=true, to_apply=%region_9.10 | all-reduce | flops 12288 | bytes 98304 | tf_op jit(solution)/shard_map/psum | solution.py:17
  68.3 2.1 broadcast_in_dim.16
  70.4 3.8 %all-to-all-start = ((bf16[4,1,192,2048]{3,2,1,0:T(8,128)(2,1)}), bf16[4,1,192,2048]{3,2,1,0:T(8,128)(2,1)S(1)}, u32[]{:S(2)}, u32[]{:S(2)}) async-start(bf16[4,1,192,2048]{3,2,1,0:T(8,128)(2,1)} %broadcast_in_dim.16), calls=%async_computation | async-start | bytes 6291456 | tf_op jit(solution)/shard_map/all_to_all | solution.py:29
  74.3 2.0 copy.54
  79.3 21.8 %all-to-all-done = bf16[4,1,192,2048]{3,2,1,0:T(8,128)(2,1)S(1)} async-done(((bf16[4,1,192,2048]{3,2,1,0:T(8,128)(2,1)}), bf16[4,1,192,2048]{3,2,1,0:T(8,128)(2,1)S(1)}, u32[]{:S(2)}, u32[]{:S(2)}) %all-to-all-start) | async-done | bytes 3145760 | tf_op jit(solution)/shard_map/all_to_all | solution.py:29
  102.8 4.1 %fusion.40 = f32[1,768,384]{1,2,0:T(8,128)S(1)} fusion(bf16[768,2048]{1,0:T(8,128)(2,1)} %bitcast.171, bf16[2048,64]{1,0:T(8,128)(2,1)} %copy.55, bf16[2048,64]{1,0:T(8,128)(2,1)} %copy.54, bf16[2048,256]{1,0:T(8,128)(2,1)} %param.25), kind=kOutput, calls=%fused_computation.46 | convolution fusion | flops 1212678144 | bytes 5898240 | tf_op jit(solution)/shard_map/srd,dc->src/dot_general | solution.py:132
  109.2 21.5 %all_gather.6 = bf16[2,1,512,64]{3,2,1,0:T(8,128)(2,1)S(1)} all-gather(bf16[2,1,32,64]{3,2,1,0:T(8,128)(2,1)S(1)} %pad_maximum_fusion.4), channel_id=1, replica_groups=mesh['sp_0'=4,'sp_1'=4,'tp'=4,'dp'=2] {'sp_0','sp_1'}, dimensions={2}, use_global_device_ids=true | all-gather | bytes 139264 | tf_op jit(solution)/shard_map/all_gather | solution.py:42
  136.5 17.2 %all-gather.2.cloned.1.call-done = bf16[2,1,12288,64]{2,3,1,0:T(8,128)(2,1)} async-done(((bf16[2,1,768,64]{2,3,1,0:T(8,128)(2,1)}), bf16[2,1,12288,64]{2,3,1,0:T(8,128)(2,1)}) %all-gather.2.cloned.1.call-update) | async-done | bytes 3145744 | tf_op jit(solution)/shard_map/all_gather | solution.py:42
  153.7 2.2 fusion.95
  157.3 93.4 %while.14 = (s32[]{:T(128)}, f32[1,1,4,768]{3,2,1,0:T(4,128)S(1)}, f32[1,1,4,768]{3,2,1,0:T(4,128)S(1)}, f32[1,1,4,768,64]{3,4,2,1,0:T(8,128)S(1)}, bf16[16,1,1,...) while((s32[]{:T(128)}, f32[1,1,4,768]{3,2,1,0:T(4,128)S(1)}, ...), condition=%wide.region_19.20_spmd, body=%wide.region_16.19_spmd.sunk | while | flops 623256576 | bytes 30671448 | solution.py:193
  157.3 2.3 bitcast_reduce_fusion.2
  159.6 1.9 fusion.113
  163.1 2.3 bitcast_reduce_fusion.2
  165.5 1.9 fusion.113
  169.0 2.3 bitcast_reduce_fusion.2
  171.3 1.9 fusion.113
  174.8 2.3 bitcast_reduce_fusion.2
  177.2 1.9 fusion.113
  180.6 2.3 bitcast_reduce_fusion.2
  183.0 1.9 fusion.113
  186.5 2.3 bitcast_reduce_fusion.2
  188.8 1.9 fusion.113
  192.3 2.3 bitcast_reduce_fusion.2
  194.7 1.9 fusion.113
  198.1 2.3 bitcast_reduce_fusion.2
  200.5 1.9 fusion.113
  204.0 2.3 bitcast_reduce_fusion.2
  206.3 1.9 fusion.113
  209.8 2.3 bitcast_reduce_fusion.2
  212.2 1.9 fusion.113
  215.7 2.3 bitcast_reduce_fusion.2
  218.0 1.9 fusion.113
  221.5 2.3 bitcast_reduce_fusion.2
  223.8 1.9 fusion.113
  227.3 2.3 bitcast_reduce_fusion.2
  229.7 1.9 fusion.113
  233.2 2.3 bitcast_reduce_fusion.2
  235.5 1.9 fusion.113
  239.0 2.3 bitcast_reduce_fusion.2
  241.3 1.9 fusion.113
  244.8 2.3 bitcast_reduce_fusion.2
  247.2 1.9 fusion.113
  252.1 3.1 %reduce.15 = bf16[768,256]{1,0:T(8,128)(2,1)S(1)} reduce(bf16[768,1,256]{2,1,0:T(2,128)(2,1)S(1)} %bitcast.172, bf16[]{:T(256)} %broadcast.434), dimensions={1}, to_apply=%bitcast.129.reduce_sub_computation | reduce | bytes 786434
  256.1 4.2 %all-to-all-start.1 = ((bf16[4,2,24576]{2,1,0:T(2,128)(2,1)}), bf16[4,2,24576]{2,1,0:T(2,128)(2,1)S(1)}, u32[]{:S(2)}, u32[]{:S(2)}) async-start(bf16[4,2,24576]{2,1,0:T(2,128)(2,1)} %reshape.681), calls=%async_computation.1 | async-start | bytes 786432 | tf_op jit(solution)/shard_map/all_to_all | solution.py:200
  260.3 7.5 %all-to-all-done.1 = bf16[4,2,24576]{2,1,0:T(2,128)(2,1)S(1)} async-done(((bf16[4,2,24576]{2,1,0:T(2,128)(2,1)}), bf16[4,2,24576]{2,1,0:T(2,128)(2,1)S(1)}, u32[]{:S(2)}, u32[]{:S(2)}) %all-to-all-start.1) | async-done | bytes 393248 | tf_op jit(solution)/shard_map/all_to_all | solution.py:200
  268.7 4.1 %fusion.28 = bf16[1,192,2048]{2,1,0:T(8,128)(2,1)} fusion(bf16[192,1024]{1,0:T(8,128)(2,1)S(1)} %bitcast.181, bf16[1024,2048]{1,0:T(8,128)(2,1)} %param.31, bf16[1,192,2048]{2,1,0:T(8,128)(2,1)S(1)} %copy-done.2, f32[2048]{0:T(1024)S(1)} %bitcast.184), kind=kOutput, calls=%fused_computation.30 | convolution fusion | flops 806879232 | bytes 6168576 | tf_op jit(solution)/shard_map/srq,qd->srd/dot_general | solution.py:198
  (160 shorter events, 49.9 us)
Async XLA Ops:
  6.5 2.1 copy-start
  70.4 5.8 %copy-start.3 = (bf16[2048,64]{0,1:T(8,128)(2,1)S(1)}, bf16[2048,64]{0,1:T(8,128)(2,1)}, u32[]{:S(2)}) copy-start(bf16[2048,64]{0,1:T(8,128)(2,1)} %param.27) | copy-start | bytes 786436
  70.4 30.7 %all-to-all-start = ((bf16[4,1,192,2048]{3,2,1,0:T(8,128)(2,1)}), bf16[4,1,192,2048]{3,2,1,0:T(8,128)(2,1)S(1)}, u32[]{:S(2)}, u32[]{:S(2)}) async-start(bf16[4,1,192,2048]{3,2,1,0:T(8,128)(2,1)} %broadcast_in_dim.16), calls=%async_computation | async-start | bytes 6291456 | tf_op jit(solution)/shard_map/all_to_all | solution.py:29
  74.2 79.4 %all-gather.2.cloned.1.call-start = ((), (), s32[]{:S(2)}) async-start(), calls=%async_computation.2 | async-start | bytes 3342336 | tf_op jit(solution)/shard_map/all_gather | solution.py:42
  101.0 1.7 copy-start.1
  102.7 4.2 %copy-start.13 = (f32[64]{0:T(128)S(1)}, f32[64]{0:T(128)}, u32[]{:S(2)}) copy-start(f32[64]{0:T(128)} %convert_element_type.131) | copy-start | bytes 772
  102.7 4.4 %copy-start.7 = (f32[1,1,768,16]{2,3,1,0:T(8,128)S(1)}, f32[1,1,768,16]{2,3,1,0:T(8,128)}, u32[]{:S(2)}) copy-start(f32[1,1,768,16]{2,3,1,0:T(8,128)} %get-tuple-element.115) | copy-start | bytes 147460
  102.7 4.4 %copy-start.8 = (f32[1,1,768,16]{2,3,1,0:T(8,128)S(1)}, f32[1,1,768,16]{2,3,1,0:T(8,128)}, u32[]{:S(2)}) copy-start(f32[1,1,768,16]{2,3,1,0:T(8,128)} %get-tuple-element.120) | copy-start | bytes 147460
  102.7 5.7 %copy-start.14 = (bf16[64]{0:T(256)(128)(2,1)S(1)}, bf16[64]{0:T(256)(128)(2,1)}, u32[]{:S(2)}) copy-start(bf16[64]{0:T(256)(128)(2,1)} %param.28) | copy-start | bytes 388
  102.7 5.7 %copy-start.9 = (bf16[1,32,2048]{2,1,0:T(8,128)(2,1)S(1)}, bf16[1,32,2048]{2,1,0:T(8,128)(2,1)}, u32[]{:S(2)}) copy-start(bf16[1,32,2048]{2,1,0:T(8,128)(2,1)} %param.20) | copy-start | bytes 393220
  102.7 5.8 %copy-start.4 = (bf16[2048,64]{0,1:T(8,128)(2,1)S(1)}, bf16[2048,64]{0,1:T(8,128)(2,1)}, u32[]{:S(2)}) copy-start(bf16[2048,64]{0,1:T(8,128)(2,1)} %param.26) | copy-start | bytes 786436
  102.7 5.8 %copy-start.10 = (f32[1,2048]{1,0:T(1,128)S(1)}, f32[1,2048]{1,0:T(1,128)}, u32[]{:S(2)}) copy-start(f32[1,2048]{1,0:T(1,128)} %get-tuple-element.124) | copy-start | bytes 24580
  106.8 23.9 %copy-start.5 = (f32[768,16]{0,1:T(8,128)S(1)}, f32[768,16]{0,1:T(8,128)}, u32[]{:S(2)}) copy-start(f32[768,16]{0,1:T(8,128)} %get-tuple-element.116) | copy-start | bytes 147460
  106.8 23.9 %copy-start.6 = (f32[768,16]{0,1:T(8,128)S(1)}, f32[768,16]{0,1:T(8,128)}, u32[]{:S(2)}) copy-start(f32[768,16]{0,1:T(8,128)} %get-tuple-element.119) | copy-start | bytes 147460
  131.4 1.3 copy-start.12
  250.7 9.6 %copy-start.11 = (f32[2,2048]{1,0:T(2,128)S(1)}, f32[2,2048]{1,0:T(2,128)}, u32[]{:S(2)}) copy-start(f32[2,2048]{1,0:T(2,128)} %get-tuple-element.89) | copy-start | bytes 49156
  252.1 16.6 %copy-start.2 = (bf16[1,192,2048]{2,1,0:T(8,128)(2,1)S(1)}, bf16[1,192,2048]{2,1,0:T(8,128)(2,1)}, u32[]{:S(2)}) copy-start(bf16[1,192,2048]{2,1,0:T(8,128)(2,1)} %param.17) | copy-start | bytes 2359300
  256.1 11.8 %all-to-all-start.1 = ((bf16[4,2,24576]{2,1,0:T(2,128)(2,1)}), bf16[4,2,24576]{2,1,0:T(2,128)(2,1)S(1)}, u32[]{:S(2)}, u32[]{:S(2)}) async-start(bf16[4,2,24576]{2,1,0:T(2,128)(2,1)} %reshape.681), calls=%async_computation.1 | async-start | bytes 786432 | tf_op jit(solution)/shard_map/all_to_all | solution.py:200
Sparse Core Ops, SparseCore 0:
  108.5 45.0 all-gather.1
where the time goes:
time: 281 us; the launch traced here: 280 us
  matrix products  81.1 us (29%)
  blocking collectives  76 us (27%)
  waiting for transfers between devices  46.5 us (17%)
  other arithmetic  38.4 us (14%)
  local copies, waits for them, and re-layouts  14.9 us (5%)
  between operations  13.9 us (5%)
  starting transfers between devices  8.12 us (3%)
    psum x3, blocking collectives, by_axis(): shard = lax.psum(shard, axis)  54.5 us
    dot_general x17, matrix products, absorb(): jnp.einsum('skgtd,skrd->skgtr', queries, key_block, preferred_element_typ...  38.1 us
    dot_general x17, matrix products, absorb(): jnp.einsum('skgtr,skrd->skgtd', weights.astype(jnp.bfloat16), value_block...  31.5 us
    reduce_sum x17, other arithmetic, absorb(): weight_sum = weight_sum * rescale + jnp.sum(weights, axis=-1)  26.1 us
    all_to_all x1, waiting for transfers between devices, copy_for_each(): return lax.all_to_all(copies, axis, split_axis=0, concat_axis=0, tiled=True)  21.8 us
    all_gather x1, blocking collectives, side_by_side(): lax.all_gather(both, axis, axis=dim, tiled=True)  21.5 us
    all_gather x1, waiting for transfers between devices, side_by_side(): lax.all_gather(both, axis, axis=dim, tiled=True)  17.2 us
    all_to_all x1, waiting for transfers between devices, on_device(): lax.all_to_all(head_rows, 'tp', split_axis=1, concat_axis=2, tiled=True)  7.5 us
  transfers between devices with their start and end apart: 3, of which 3 were waited for; matrix products, arithmetic and copies ran while one was open for 4% of the time, Pallas kernels for 0%

commit v1 on v0

--- a/solution.py
+++ b/solution.py
@@ -14,7 +14,7 @@
 
 def by_axis(shard, axes):
     for axis in axes:
-        shard = lax.psum(shard, axis)
+        shard = jnp.sum(lax.all_gather(shard, axis), axis=0)
     return shard
 
 

time: 281 us -> 326 us (1.16)
  blocking collectives: 76 us -> 134 us
  waiting for transfers between devices: 46.5 us -> 33.8 us
    all_gather x0 -> x9, blocking collectives: none -> 110 us  [by_axis(): shard = jnp.sum(lax.all_gather(shard, axis), axis=0)]
    psum x3 -> x0, blocking collectives: 54.5 us -> none  [by_axis(): shard = lax.psum(shard, axis)]
    all_to_all x1, waiting for transfers between devices: 7.5 us -> 0.01 us  [on_device(): lax.all_to_all(head_rows, 'tp', split_axis=1, concat_axis=2, tiled=True)]
    all_to_all x1, waiting for transfers between devices: 21.8 us -> 17.1 us  [copy_for_each(): return lax.all_to_all(copies, axis, split_axis=0, concat_axis=0, tiled=True)]
    unnamed x37 -> x41, local copies, waits for them, and re-layouts: 6.55 us -> 7.48 us
  transfers between devices with their start and end apart: 3 -> 3, of which waited for: 3 -> 2; matrix products, arithmetic and copies ran while one was open for 4% -> 4% of each run, Pallas kernels for 0% -> 0%
where the time goes in v1:
time: 326 us; the launch traced here: 325 us
  blocking collectives  134 us (41%)
  matrix products  80.1 us (25%)
  other arithmetic  38 us (12%)
  waiting for transfers between devices  33.8 us (10%)
  local copies, waits for them, and re-layouts  16.4 us (5%)
  between operations  13.9 us (4%)
  starting transfers between devices  8.12 us (2%)
    all_gather x9, blocking collectives, by_axis(): shard = jnp.sum(lax.all_gather(shard, axis), axis=0)  110 us
    dot_general x17, matrix products, absorb(): jnp.einsum('skgtd,skrd->skgtr', queries, key_block, preferred_element_typ...  38.1 us
    dot_general x17, matrix products, absorb(): jnp.einsum('skgtr,skrd->skgtd', weights.astype(jnp.bfloat16), value_block...  31.5 us
    reduce_sum x17, other arithmetic, absorb(): weight_sum = weight_sum * rescale + jnp.sum(weights, axis=-1)  26.1 us
    all_gather x1, blocking collectives, side_by_side(): lax.all_gather(both, axis, axis=dim, tiled=True)  23.8 us
    all_to_all x1, waiting for transfers between devices, copy_for_each(): return lax.all_to_all(copies, axis, split_axis=0, concat_axis=0, tiled=True)  17.1 us
    all_gather x1, waiting for transfers between devices, side_by_side(): lax.all_gather(both, axis, axis=dim, tiled=True)  16.7 us
    unnamed x41, local copies, waits for them, and re-layouts  7.48 us
  transfers between devices with their start and end apart: 3, of which 2 were waited for; matrix products, arithmetic and copies ran while one was open for 4% of the time, Pallas kernels for 0%

profile of v1, /device:TPU:0, one launch (start us, length us, event | category | flops | bytes accessed | tf_op | source)
XLA Modules:
  0.0 324.9 jit_solution(5699073884801810827)
XLA Ops:
  8.2 13.2 %all_gather.67 = f32[4,2,2048]{2,1,0:T(2,128)S(1)} all-gather(f32[1,2,2048]{2,1,0:T(2,128)S(1)} %fusion.50), channel_id=1, replica_groups=mesh['sp_0'=4,'sp_1'=4,'tp'=4,'dp'=2] {'sp_0'}, dimensions={0}, use_global_device_ids=true | all-gather | bytes 81920 | tf_op jit(solution)/shard_map/all_gather | solution.py:17
  21.5 12.4 %all-gather.8 = f32[4,2,2048]{2,1,0:T(2,128)S(1)} all-gather(f32[1,2,2048]{2,1,0:T(2,128)S(1)} %bitcast.200), channel_id=4, replica_groups=mesh['sp_0'=4,'sp_1'=4,'tp'=4,'dp'=2] {'sp_1'}, dimensions={0}, use_global_device_ids=true | all-gather | bytes 81920 | tf_op jit(solution)/shard_map/all_gather | solution.py:17
  33.9 12.2 %all-gather.9 = f32[4,2,2048]{2,1,0:T(2,128)S(1)} all-gather(f32[1,2,2048]{2,1,0:T(2,128)S(1)} %bitcast.201), channel_id=5, replica_groups=mesh['sp_0'=4,'sp_1'=4,'tp'=4,'dp'=2] {'tp'}, dimensions={0}, use_global_device_ids=true | all-gather | bytes 81920 | tf_op jit(solution)/shard_map/all_gather | solution.py:17
  47.2 11.9 %all_gather.73 = f32[4,2,2048]{2,1,0:T(2,128)S(1)} all-gather(f32[1,2,2048]{2,1,0:T(2,128)S(1)} %fusion.49), channel_id=1, replica_groups=mesh['sp_0'=4,'sp_1'=4,'tp'=4,'dp'=2] {'sp_0'}, dimensions={0}, use_global_device_ids=true | all-gather | bytes 81920 | tf_op jit(solution)/shard_map/all_gather | solution.py:17
  59.1 11.9 %all-gather.10 = f32[4,2,2048]{2,1,0:T(2,128)S(1)} all-gather(f32[1,2,2048]{2,1,0:T(2,128)S(1)} %bitcast.202), channel_id=6, replica_groups=mesh['sp_0'=4,'sp_1'=4,'tp'=4,'dp'=2] {'sp_1'}, dimensions={0}, use_global_device_ids=true | all-gather | bytes 81920 | tf_op jit(solution)/shard_map/all_gather | solution.py:17
  71.0 12.0 %all-gather.11 = f32[4,2,2048]{2,1,0:T(2,128)S(1)} all-gather(f32[1,2,2048]{2,1,0:T(2,128)S(1)} %bitcast.203), channel_id=7, replica_groups=mesh['sp_0'=4,'sp_1'=4,'tp'=4,'dp'=2] {'tp'}, dimensions={0}, use_global_device_ids=true | all-gather | bytes 81920 | tf_op jit(solution)/shard_map/all_gather | solution.py:17
  87.2 2.1 broadcast_in_dim.16
  89.3 3.8 %all-to-all-start = ((bf16[4,1,192,2048]{3,2,1,0:T(8,128)(2,1)}), bf16[4,1,192,2048]{3,2,1,0:T(8,128)(2,1)S(1)}, u32[]{:S(2)}, u32[]{:S(2)}) async-start(bf16[4,1,192,2048]{3,2,1,0:T(8,128)(2,1)} %broadcast_in_dim.16), calls=%async_computation | async-start | bytes 6291456 | tf_op jit(solution)/shard_map/all_to_all | solution.py:29
  93.2 2.0 copy.54
  98.1 17.1 %all-to-all-done = bf16[4,1,192,2048]{3,2,1,0:T(8,128)(2,1)S(1)} async-done(((bf16[4,1,192,2048]{3,2,1,0:T(8,128)(2,1)}), bf16[4,1,192,2048]{3,2,1,0:T(8,128)(2,1)S(1)}, u32[]{:S(2)}, u32[]{:S(2)}) %all-to-all-start) | async-done | bytes 3145760 | tf_op jit(solution)/shard_map/all_to_all | solution.py:29
  116.9 4.1 %fusion.40 = f32[1,768,384]{1,2,0:T(8,128)S(1)} fusion(bf16[768,2048]{1,0:T(8,128)(2,1)} %bitcast.189, bf16[2048,64]{1,0:T(8,128)(2,1)} %copy.55, bf16[2048,64]{1,0:T(8,128)(2,1)} %copy.54, bf16[2048,256]{1,0:T(8,128)(2,1)} %param.25), kind=kOutput, calls=%fused_computation.46 | convolution fusion | flops 1212678144 | bytes 5898240 | tf_op jit(solution)/shard_map/srd,dc->src/dot_general | solution.py:132
  123.4 23.8 %all_gather.78 = bf16[2,1,512,64]{3,2,1,0:T(8,128)(2,1)S(1)} all-gather(bf16[2,1,32,64]{3,2,1,0:T(8,128)(2,1)S(1)} %pad_maximum_fusion.4), channel_id=1, replica_groups=mesh['sp_0'=4,'sp_1'=4,'tp'=4,'dp'=2] {'sp_0','sp_1'}, dimensions={2}, use_global_device_ids=true | all-gather | bytes 139264 | tf_op jit(solution)/shard_map/all_gather | solution.py:42
  153.0 16.7 %all-gather.14.cloned.1.call-done = bf16[2,1,12288,64]{2,3,1,0:T(8,128)(2,1)} async-done(((bf16[2,1,768,64]{2,3,1,0:T(8,128)(2,1)}), bf16[2,1,12288,64]{2,3,1,0:T(8,128)(2,1)}) %all-gather.14.cloned.1.call-update) | async-done | bytes 3145744 | tf_op jit(solution)/shard_map/all_gather | solution.py:42
  169.8 2.2 fusion.98
  173.4 93.4 %while.14 = (s32[]{:T(128)}, f32[1,1,4,768]{3,2,1,0:T(4,128)S(1)}, f32[1,1,4,768]{3,2,1,0:T(4,128)S(1)}, f32[1,1,4,768,64]{3,4,2,1,0:T(8,128)S(1)}, bf16[16,1,1,...) while((s32[]{:T(128)}, f32[1,1,4,768]{3,2,1,0:T(4,128)S(1)}, ...), condition=%wide.region_19.20_spmd, body=%wide.region_16.19_spmd.sunk | while | flops 623256576 | bytes 30671448 | solution.py:193
  173.4 2.3 bitcast_reduce_fusion.2
  175.7 1.9 fusion.116
  179.2 2.3 bitcast_reduce_fusion.2
  181.6 1.9 fusion.116
  185.1 2.3 bitcast_reduce_fusion.2
  187.4 1.9 fusion.116
  190.9 2.3 bitcast_reduce_fusion.2
  193.3 1.9 fusion.116
  196.7 2.3 bitcast_reduce_fusion.2
  199.1 1.9 fusion.116
  202.6 2.3 bitcast_reduce_fusion.2
  204.9 1.9 fusion.116
  208.4 2.3 bitcast_reduce_fusion.2
  214.2 2.3 bitcast_reduce_fusion.2
  216.6 1.9 fusion.116
  220.1 2.3 bitcast_reduce_fusion.2
  225.9 2.3 bitcast_reduce_fusion.2
  228.3 1.9 fusion.116
  231.8 2.3 bitcast_reduce_fusion.2
  237.6 2.3 bitcast_reduce_fusion.2
  239.9 1.9 fusion.116
  243.4 2.3 bitcast_reduce_fusion.2
  249.3 2.3 bitcast_reduce_fusion.2
  251.6 1.9 fusion.116
  255.1 2.3 bitcast_reduce_fusion.2
  260.9 2.3 bitcast_reduce_fusion.2
  263.3 1.9 fusion.116
  268.2 3.0 reduce.21
  272.1 4.2 %all-to-all-start.1 = ((bf16[4,2,24576]{2,1,0:T(2,128)(2,1)}), bf16[4,2,24576]{2,1,0:T(2,128)(2,1)S(1)}, u32[]{:S(2)}, u32[]{:S(2)}) async-start(bf16[4,2,24576]{2,1,0:T(2,128)(2,1)} %reshape.711), calls=%async_computation.1 | async-start | bytes 786432 | tf_op jit(solution)/shard_map/all_to_all | solution.py:200
  276.5 11.9 %all_gather.61 = f32[4,2,2048]{2,1,0:T(2,128)S(1)} all-gather(f32[1,2,2048]{2,1,0:T(2,128)S(1)} %fusion.51), channel_id=1, replica_groups=mesh['sp_0'=4,'sp_1'=4,'tp'=4,'dp'=2] {'sp_0'}, dimensions={0}, use_global_device_ids=true | all-gather | bytes 81920 | tf_op jit(solution)/shard_map/all_gather | solution.py:17
  288.4 11.9 %all-gather.6 = f32[4,2,2048]{2,1,0:T(2,128)S(1)} all-gather(f32[1,2,2048]{2,1,0:T(2,128)S(1)} %bitcast.204), channel_id=2, replica_groups=mesh['sp_0'=4,'sp_1'=4,'tp'=4,'dp'=2] {'sp_1'}, dimensions={0}, use_global_device_ids=true | all-gather | bytes 81920 | tf_op jit(solution)/shard_map/all_gather | solution.py:17
  300.4 12.7 %all-gather.7 = f32[4,2,2048]{2,1,0:T(2,128)S(1)} all-gather(f32[1,2,2048]{2,1,0:T(2,128)S(1)} %bitcast.205), channel_id=3, replica_groups=mesh['sp_0'=4,'sp_1'=4,'tp'=4,'dp'=2] {'tp'}, dimensions={0}, use_global_device_ids=true | all-gather | bytes 81920 | tf_op jit(solution)/shard_map/all_gather | solution.py:17
  314.0 4.1 %fusion.28 = bf16[1,192,2048]{2,1,0:T(8,128)(2,1)} fusion(bf16[192,1024]{1,0:T(8,128)(2,1)S(1)} %bitcast.199, bf16[1024,2048]{1,0:T(8,128)(2,1)} %param.31, bf16[1,192,2048]{2,1,0:T(8,128)(2,1)S(1)} %copy-done.2, f32[2048]{0:T(1024)S(1)} %bitcast.208), kind=kOutput, calls=%fused_computation.30 | convolution fusion | flops 806879232 | bytes 6168576 | tf_op jit(solution)/shard_map/srq,qd->srd/dot_general | solution.py:198
  (180 shorter events, 59.5 us)
Async XLA Ops:
  6.5 0.9 copy-start
  89.3 5.8 %copy-start.3 = (bf16[2048,64]{0,1:T(8,128)(2,1)S(1)}, bf16[2048,64]{0,1:T(8,128)(2,1)}, u32[]{:S(2)}) copy-start(bf16[2048,64]{0,1:T(8,128)(2,1)} %param.27) | copy-start | bytes 786436
  89.3 25.9 %all-to-all-start = ((bf16[4,1,192,2048]{3,2,1,0:T(8,128)(2,1)}), bf16[4,1,192,2048]{3,2,1,0:T(8,128)(2,1)S(1)}, u32[]{:S(2)}, u32[]{:S(2)}) async-start(bf16[4,1,192,2048]{3,2,1,0:T(8,128)(2,1)} %broadcast_in_dim.16), calls=%async_computation | async-start | bytes 6291456 | tf_op jit(solution)/shard_map/all_to_all | solution.py:29
  93.1 76.6 %all-gather.14.cloned.1.call-start = ((), (), s32[]{:S(2)}) async-start(), calls=%async_computation.2 | async-start | bytes 3342336 | tf_op jit(solution)/shard_map/all_gather | solution.py:42
  115.2 1.7 copy-start.1
  116.9 4.2 %copy-start.15 = (f32[64]{0:T(128)S(1)}, f32[64]{0:T(128)}, u32[]{:S(2)}) copy-start(f32[64]{0:T(128)} %convert_element_type.131) | copy-start | bytes 772
  116.9 4.4 %copy-start.7 = (f32[1,1,768,16]{2,3,1,0:T(8,128)S(1)}, f32[1,1,768,16]{2,3,1,0:T(8,128)}, u32[]{:S(2)}) copy-start(f32[1,1,768,16]{2,3,1,0:T(8,128)} %get-tuple-element.106) | copy-start | bytes 147460
  116.9 4.4 %copy-start.8 = (f32[1,1,768,16]{2,3,1,0:T(8,128)S(1)}, f32[1,1,768,16]{2,3,1,0:T(8,128)}, u32[]{:S(2)}) copy-start(f32[1,1,768,16]{2,3,1,0:T(8,128)} %get-tuple-element.111) | copy-start | bytes 147460
  116.9 5.7 %copy-start.16 = (bf16[64]{0:T(256)(128)(2,1)S(1)}, bf16[64]{0:T(256)(128)(2,1)}, u32[]{:S(2)}) copy-start(bf16[64]{0:T(256)(128)(2,1)} %param.28) | copy-start | bytes 388
  116.9 5.7 %copy-start.9 = (bf16[1,32,2048]{2,1,0:T(8,128)(2,1)S(1)}, bf16[1,32,2048]{2,1,0:T(8,128)(2,1)}, u32[]{:S(2)}) copy-start(bf16[1,32,2048]{2,1,0:T(8,128)(2,1)} %param.20) | copy-start | bytes 393220
  116.9 5.8 %copy-start.4 = (bf16[2048,64]{0,1:T(8,128)(2,1)S(1)}, bf16[2048,64]{0,1:T(8,128)(2,1)}, u32[]{:S(2)}) copy-start(bf16[2048,64]{0,1:T(8,128)(2,1)} %param.26) | copy-start | bytes 786436
  116.9 5.8 %copy-start.11 = (f32[1,2048]{1,0:T(1,128)S(1)}, f32[1,2048]{1,0:T(1,128)}, u32[]{:S(2)}) copy-start(f32[1,2048]{1,0:T(1,128)} %get-tuple-element.101) | copy-start | bytes 24580
  121.0 26.2 %copy-start.5 = (f32[768,16]{0,1:T(8,128)S(1)}, f32[768,16]{0,1:T(8,128)}, u32[]{:S(2)}) copy-start(f32[768,16]{0,1:T(8,128)} %get-tuple-element.107) | copy-start | bytes 147460
  121.0 26.2 %copy-start.6 = (f32[768,16]{0,1:T(8,128)S(1)}, f32[768,16]{0,1:T(8,128)}, u32[]{:S(2)}) copy-start(f32[768,16]{0,1:T(8,128)} %get-tuple-element.110) | copy-start | bytes 147460
  147.9 1.3 copy-start.14
  266.8 9.6 %copy-start.10 = (bf16[128,512]{1,0:T(8,128)(2,1)S(1)}, bf16[128,512]{1,0:T(8,128)(2,1)}, u32[]{:S(2)}) copy-start(bf16[128,512]{1,0:T(8,128)(2,1)} %param.24) | copy-start | bytes 393220
  266.8 9.6 %copy-start.12 = (bf16[128]{0:T(256)(128)(2,1)S(1)}, bf16[128]{0:T(256)(128)(2,1)}, u32[]{:S(2)}) copy-start(bf16[128]{0:T(256)(128)(2,1)} %param.19) | copy-start | bytes 772
  266.8 9.6 %copy-start.13 = (bf16[1,128]{1,0:T(2,128)(2,1)S(1)}, bf16[1,128]{1,0:T(2,128)(2,1)}, u32[]{:S(2)}) copy-start(bf16[1,128]{1,0:T(2,128)(2,1)} %param.18) | copy-start | bytes 772
  271.3 42.7 %copy-start.2 = (bf16[1,192,2048]{2,1,0:T(8,128)(2,1)S(1)}, bf16[1,192,2048]{2,1,0:T(8,128)(2,1)}, u32[]{:S(2)}) copy-start(bf16[1,192,2048]{2,1,0:T(8,128)(2,1)} %param.17) | copy-start | bytes 2359300
  272.1 41.0 %all-to-all-start.1 = ((bf16[4,2,24576]{2,1,0:T(2,128)(2,1)}), bf16[4,2,24576]{2,1,0:T(2,128)(2,1)S(1)}, u32[]{:S(2)}, u32[]{:S(2)}) async-start(bf16[4,2,24576]{2,1,0:T(2,128)(2,1)} %reshape.711), calls=%async_computation.1 | async-start | bytes 786432 | tf_op jit(solution)/shard_map/all_to_all | solution.py:200
Sparse Core Ops, SparseCore 0:
  122.7 47.0 all-gather.13
